TPU v7x, 32 devices: a whole 2x2x4 slice. The times are simulated.
32 devices in a mesh: ra: 4 (over z), cb: 4 (over y, x), dp: 2 (over core).
Axes of the slice: x: 2, y: 2, z: 4, core: 2. Of those that a mesh axis runs over, the one named last changes fastest.
Arguments:
- tokens: bfloat16 [2, 512, 4096], P('dp', None, 'ra'), may hold values from -80 to 80
- pre_gain: float32 [4096], P('ra'), may hold values from 0.1 to 1.9
- w_gate: bfloat16 [4096, 11264], P('ra', 'cb'), may hold values from -0.09375 to 0.09375
- w_up: bfloat16 [4096, 11264], P('ra', 'cb'), may hold values from -0.09375 to 0.09375
- conv_gate: float32 [3, 11264], P(None, 'cb'), may hold values from -3.5 to 3.5
- conv_up: float32 [3, 11264], P(None, 'cb'), may hold values from -3.5 to 3.5
- w_down: bfloat16 [11264, 4096], P('cb', 'ra'), may hold values from -2 to 2
- post_gain: float32 [4096], P('ra'), may hold values from 0.1 to 1.9
Outputs:
- mixed: bfloat16 [2, 512, 4096], P('dp', None, 'ra')
All inputs are finite; a program needn't handle non-finite values.
Results may differ from a plain program's by a relative error of at most 0.0064.
Values may be sent and summed in bfloat16 or wider, within the bound.
A program may use at most 128 MiB of HBM per device.

v0:
```python
import jax
import jax.numpy as jnp
from jax import lax
from jax.sharding import PartitionSpec as P

epsilon = 1e-06
residual_scale = 0.125


def convolve(field, tap_weights):
    zero_col = jnp.zeros((field.shape[0], 1), jnp.float32)
    before = jnp.concatenate([zero_col, field[:, :-1]], axis=1)
    later_cols = jnp.concatenate([field[:, 1:], zero_col], axis=1)
    return (
        tap_weights[0][:, None] * before
        + tap_weights[1][:, None] * field
        + tap_weights[2][:, None] * later_cols
    )


def local(tokens, pre_gain, w_gate, w_up, conv_gate, conv_up, w_down, post_gain):
    ra_count = lax.axis_size("ra")
    dim_full = tokens.shape[2] * ra_count
    values = tokens[0].astype(jnp.float32)
    local_sq = jnp.sum(values * values, axis=1)
    total_sq = lax.psum(local_sq, "ra")
    in_scale = lax.rsqrt(total_sq / dim_full + epsilon)
    weighted = (values * pre_gain).astype(jnp.bfloat16)
    gate_cols, up_cols = (
        lax.all_to_all(w_gate, "ra", split_axis=1, concat_axis=0, tiled=True),
        lax.all_to_all(w_up, "ra", split_axis=1, concat_axis=0, tiled=True),
    )
    own_units = gate_cols.shape[1]
    piece = lax.all_gather(weighted, "ra", axis=1, tiled=True)
    dims = (((0,), (1,)), ((), ()))
    gate_sum = lax.dot_general(gate_cols, piece, dims, preferred_element_type=jnp.float32)
    up_sum = lax.dot_general(up_cols, piece, dims, preferred_element_type=jnp.float32)
    offset_units = lax.axis_index("ra") * own_units
    taps_gate = lax.dynamic_slice_in_dim(conv_gate, offset_units, own_units, 1)
    taps_up = lax.dynamic_slice_in_dim(conv_up, offset_units, own_units, 1)
    gate_lin = gate_sum * in_scale[None, :]
    up_lin = up_sum * in_scale[None, :]
    hidden = (
        jax.nn.gelu(convolve(gate_lin, taps_gate), approximate=True) * convolve(up_lin, taps_up)
    ).astype(jnp.bfloat16)
    partial_value = lax.dot_general(
        lax.all_gather(hidden, "ra", axis=0, tiled=True),
        w_down,
        (((0,), (0,)), ((), ())),
        preferred_element_type=jnp.float32,
    )
    branch = lax.psum(partial_value, "cb")
    post_sq = lax.psum(jnp.sum(branch * branch, axis=1), "ra")
    post_scale = lax.rsqrt(post_sq / dim_full + epsilon)
    mixed = residual_scale * values + branch * post_scale[:, None] * post_gain
    return mixed.astype(jnp.bfloat16)[None]


def solution(mesh):
    in_specs = (
        P("dp", None, "ra"),
        P("ra"),
        P("ra", "cb"),
        P("ra", "cb"),
        P(None, "cb"),
        P(None, "cb"),
        P("cb", "ra"),
        P("ra"),
    )
    out_specs = P("dp", None, "ra")
    return jax.shard_map(local, mesh=mesh, in_specs=in_specs, out_specs=out_specs, check_vma=False)
```

profile of v0, /device:TPU:0, one launch (start us, length us, event | category | flops | bytes accessed | tf_op | source)
XLA Modules:
  0.0 532.4 jit_solution(12061142635943834656)
XLA Ops:
  6.5 8.3 %copy.11 = bf16[1024,2816]{0,1:T(8,128)(2,1)} copy(bf16[1024,2816]{1,0:T(8,128)(2,1)} %param.11) | data formatting | bytes 11534336 | tf_op args[3]
  14.8 6.3 %all-to-all-start.1 = ((bf16[1024,4,704]{0,2,1:T(8,128)(2,1)}), bf16[1024,4,704]{0,2,1:T(8,128)(2,1)}, u32[]{:S(2)}, u32[]{:S(2)}) async-start(bf16[1024,4,704]{0,2,1:T(8,128)(2,1)} %bitcast.26), calls=%async_computation.1 | async-start | bytes 11534336 | tf_op jit(solution)/shard_map/all_to_all | solution.py:31
  21.1 8.3 %copy.9 = bf16[1024,2816]{0,1:T(8,128)(2,1)} copy(bf16[1024,2816]{1,0:T(8,128)(2,1)} %param.10) | data formatting | bytes 11534336 | tf_op args[2]
  29.5 119.1 %all-to-all-done.1 = bf16[1024,4,704]{0,2,1:T(8,128)(2,1)} async-done(((bf16[1024,4,704]{0,2,1:T(8,128)(2,1)}), bf16[1024,4,704]{0,2,1:T(8,128)(2,1)}, u32[]{:S(2)}, u32[]{:S(2)}) %all-to-all-start.1) | async-done | bytes 5767200 | tf_op jit(solution)/shard_map/all_to_all | solution.py:31
  148.6 5.3 all-to-all-start
  154.0 1.3 fusion.3
  155.3 0.0 all-gather.5.cloned.1.call-start
  155.3 1.0 dynamic-slice_reduce_fusion.2
  156.3 163.7 %psum.21 = f32[512]{0:T(512)S(1)} all-reduce(f32[512]{0:T(512)S(1)} %get-tuple-element.15), channel_id=1, replica_groups=mesh['ra'=4,'cb'=4,'dp'=2] {'ra'}, use_global_device_ids=true, to_apply=%region_1.0 | all-reduce | flops 512 | bytes 4096 | tf_op jit(solution)/shard_map/psum | solution.py:26
  320.0 6.1 %copy.14 = bf16[4,88,8,1024]{3,2,0,1:T(8,128)(2,1)} copy(bf16[4,88,8,1024]{3,2,1,0:T(8,128)(2,1)} %bitcast.11) | data formatting | bytes 11534336 | tf_op jit(solution)/shard_map/all_to_all | solution.py:31
  326.1 22.0 %all-to-all-done = bf16[1024,4,704]{0,2,1:T(8,128)(2,1)} async-done(((bf16[1024,4,704]{0,2,1:T(8,128)(2,1)}), bf16[1024,4,704]{0,2,1:T(8,128)(2,1)}, u32[]{:S(2)}, u32[]{:S(2)}) %all-to-all-start) | async-done | bytes 5767200 | tf_op jit(solution)/shard_map/all_to_all | solution.py:30
  348.1 6.1 %copy.13 = bf16[4,88,8,1024]{3,2,0,1:T(8,128)(2,1)} copy(bf16[4,88,8,1024]{3,2,1,0:T(8,128)(2,1)} %bitcast.9) | data formatting | bytes 11534336 | tf_op jit(solution)/shard_map/all_to_all | solution.py:30
  354.3 6.6 %fusion.4 = f32[704,512]{1,0:T(8,128)S(1)} fusion(bf16[512,4096]{1,0:T(8,128)(2,1)} %all-gather.3.cloned.1.call-done, bf16[4096,704]{0,1:T(8,128)(2,1)} %bitcast.27, f32[512]{0:T(512)S(1)} %add_rsqrt_fusion.1), kind=kOutput, calls=%fused_computation.10 | convolution fusion | flops 2953150464 | bytes 11405312 | tf_op jit(solution)/shard_map/dot_general | solution.py:37
  360.9 0.1 copy-done.5
  361.0 3.2 fusion.5
  364.2 1.0 fusion.16
  365.2 2.8 fusion.14
  368.0 0.0 all-reduce.6.cloned.1.call-start
  368.1 66.4 %all-gather.5.cloned.1.call-done = bf16[2816,512]{1,0:T(8,128)(2,1)} async-done(((bf16[704,512]{1,0:T(8,128)(2,1)}), bf16[2816,512]{1,0:T(8,128)(2,1)}) %all-gather.5.cloned.1.call-update) | async-done | bytes 2883600 | tf_op jit(solution)/shard_map/all_gather | solution.py:47
  434.5 8.0 %fusion.18 = f32[512,1024]{1,0:T(8,128)} fusion(bf16[2816,512]{1,0:T(8,128)(2,1)} %all-gather.5.cloned.1.call-done, bf16[2816,1024]{1,0:T(8,128)(2,1)} %param.14), kind=kOutput, calls=%fused_computation.33 | convolution fusion | flops 2952790016 | bytes 10747904 | tf_op jit(solution)/shard_map/dot_general | solution.py:46
  442.5 68.3 %all-reduce.6.cloned.1.call-done = f32[512,1024]{1,0:T(8,128)} async-done(((f32[512,1024]{1,0:T(8,128)}), f32[512,1024]{1,0:T(8,128)}) %all-reduce.6.cloned.1.call-update) | async-done | bytes 2097168 | tf_op jit(solution)/shard_map/psum | solution.py:52
  510.8 2.0 multiply_reduce_fusion
  512.8 11.7 %psum.23 = f32[512]{0:T(512)S(1)} all-reduce(f32[512]{0:T(512)S(1)} %multiply_reduce_fusion), channel_id=1, replica_groups=mesh['ra'=4,'cb'=4,'dp'=2] {'ra'}, use_global_device_ids=true, to_apply=%region_4.0 | all-reduce | flops 512 | bytes 4096 | tf_op jit(solution)/shard_map/psum | solution.py:53
  524.5 1.4 fusion.15
  (18 shorter events, 0.1 us)
Async XLA Ops:
  14.8 133.8 %all-to-all-start.1 = ((bf16[1024,4,704]{0,2,1:T(8,128)(2,1)}), bf16[1024,4,704]{0,2,1:T(8,128)(2,1)}, u32[]{:S(2)}, u32[]{:S(2)}) async-start(bf16[1024,4,704]{0,2,1:T(8,128)(2,1)} %bitcast.26), calls=%async_computation.1 | async-start | bytes 11534336 | tf_op jit(solution)/shard_map/all_to_all | solution.py:31
  148.6 5.3 %copy-start.2 = (bf16[1,512,1024]{2,1,0:T(8,128)(2,1)S(1)}, bf16[1,512,1024]{2,1,0:T(8,128)(2,1)}, u32[]{:S(2)}) copy-start(bf16[1,512,1024]{2,1,0:T(8,128)(2,1)} %param.8) | copy-start | bytes 3145732
  148.6 5.4 %copy-start.3 = (f32[1024]{0:T(1024)S(1)}, f32[1024]{0:T(1024)}, u32[]{:S(2)}) copy-start(f32[1024]{0:T(1024)} %param.9) | copy-start | bytes 12292
  148.6 199.5 %all-to-all-start = ((bf16[1024,4,704]{0,2,1:T(8,128)(2,1)}), bf16[1024,4,704]{0,2,1:T(8,128)(2,1)}, u32[]{:S(2)}, u32[]{:S(2)}) async-start(bf16[1024,4,704]{0,2,1:T(8,128)(2,1)} %bitcast.25), calls=%async_computation | async-start | bytes 11534336 | tf_op jit(solution)/shard_map/all_to_all | solution.py:30
  153.9 200.4 %all-gather.3.cloned.1.call-start = ((), (), s32[]{:S(2)}) async-start(), calls=%async_computation.2 | async-start | bytes 5242880 | tf_op jit(solution)/shard_map/all_gather | solution.py:34
  155.3 279.2 %all-gather.5.cloned.1.call-start = ((), (), s32[]{:S(2)}) async-start(), calls=%async_computation.3 | async-start | bytes 3604480 | tf_op jit(solution)/shard_map/all_gather | solution.py:47
  354.3 6.6 %copy-start.1 = (bf16[4,88,8,1024]{3,2,0,1:T(8,128)(2,1)S(1)}, bf16[4,88,8,1024]{3,2,0,1:T(8,128)(2,1)}, u32[]{:S(2)}) copy-start(bf16[4,88,8,1024]{3,2,0,1:T(8,128)(2,1)} %copy.13) | copy-start | bytes 17301508
  354.3 6.8 %copy-start.5 = (bf16[512,4096]{1,0:T(8,128)(2,1)S(1)}, bf16[512,4096]{1,0:T(8,128)(2,1)}, u32[]{:S(2)}) copy-start(bf16[512,4096]{1,0:T(8,128)(2,1)} %all-gather.3.cloned.1.call-done) | copy-start | bytes 12582916
  368.0 142.8 %all-reduce.6.cloned.1.call-start = ((), (), s32[]{:S(2)}) async-start(), calls=%async_computation.4 | async-start | bytes 4194304 | tf_op jit(solution)/shard_map/psum | solution.py:52
  442.5 82.0 %copy-start.4 = (f32[1024]{0:T(1024)S(1)}, f32[1024]{0:T(1024)}, u32[]{:S(2)}) copy-start(f32[1024]{0:T(1024)} %param.15) | copy-start | bytes 12292
  510.8 13.7 %copy-start = (f32[512,1024]{1,0:T(8,128)S(1)}, f32[512,1024]{1,0:T(8,128)}, u32[]{:S(2)}) copy-start(f32[512,1024]{1,0:T(8,128)} %all-reduce.6.cloned.1.call-done) | copy-start | bytes 6291460
Sparse Core Ops, SparseCore 0:
  156.3 164.8 all-gather.2
  368.2 66.2 all-gather.4
  442.6 68.1 all-reduce.5
where the time goes:
time: 533 us; the launch traced here: 532 us
  waiting for transfers between devices  276 us (52%)
  blocking collectives  175 us (33%)
  local copies, waits for them, and re-layouts  31 us (6%)
  matrix products  17.8 us (3%)
  between operations  13.2 us (2%)
  starting transfers between devices  11.8 us (2%)
  other arithmetic  7.39 us (1%)
    psum x1, blocking collectives, local(): total_sq = lax.psum(local_sq, 'ra')  164 us
    all_to_all x1, waiting for transfers between devices, local(): lax.all_to_all(w_up, 'ra', split_axis=1, concat_axis=0, tiled=True)  119 us
    psum x1, waiting for transfers between devices, local(): branch = lax.psum(partial_value, 'cb')  68.3 us
    all_gather x1, waiting for transfers between devices, local(): lax.all_gather(hidden, 'ra', axis=0, tiled=True)  66.4 us
    all_to_all x1, waiting for transfers between devices, local(): lax.all_to_all(w_gate, 'ra', split_axis=1, concat_axis=0, tiled=True)  22 us
    unnamed x14, local copies, waits for them, and re-layouts  16.7 us
    psum x1, blocking collectives, local(): post_sq = lax.psum(jnp.sum(branch * branch, axis=1), 'ra')  11.7 us
  transfers between devices with their start and end apart: 5, of which 4 were waited for; matrix products, arithmetic and copies ran while one was open for 4% of the time, Pallas kernels for 0%

commit v1 on v0

--- a/solution.py
+++ b/solution.py
@@ -49,7 +49,9 @@
         (((0,), (0,)), ((), ())),
         preferred_element_type=jnp.float32,
     )
-    branch = lax.psum(partial_value, "cb")
+    branch = partial_value
+    for hop in (1, 2):
+        branch = branch + lax.ppermute(branch, "cb", [(dev, dev ^ hop) for dev in range(4)])
     post_sq = lax.psum(jnp.sum(branch * branch, axis=1), "ra")
     post_scale = lax.rsqrt(post_sq / dim_full + epsilon)
     mixed = residual_scale * values + branch * post_scale[:, None] * post_gain

time: 533 us -> 554 us (1.039)
  waiting for transfers between devices: 276 us -> 298 us
    ppermute x0 -> x2, waiting for transfers between devices: none -> 90.6 us  [local(): lax.ppermute(branch, 'cb', [(dev, dev ^ hop) for dev in range(4)])]
    psum x1 -> x0, waiting for transfers between devices: 68.3 us -> none  [local(): branch = lax.psum(partial_value, 'cb')]
    unnamed x14 -> x12, local copies, waits for them, and re-layouts: 16.7 us -> 16.7 us
  transfers between devices with their start and end apart: 5 -> 6, of which waited for: 4 -> 5; matrix products, arithmetic and copies ran while one was open for 4% -> 4% of each run, Pallas kernels for 0% -> 0%
where the time goes in v1:
time: 554 us; the launch traced here: 553 us
  waiting for transfers between devices  298 us (54%)
  blocking collectives  174 us (31%)
  local copies, waits for them, and re-layouts  31 us (6%)
  matrix products  15.9 us (3%)
  starting transfers between devices  14.8 us (3%)
  between operations  13.5 us (2%)
  other arithmetic  6.29 us (1%)
    psum x1, blocking collectives, local(): total_sq = lax.psum(local_sq, 'ra')  164 us
    all_to_all x1, waiting for transfers between devices, local(): lax.all_to_all(w_up, 'ra', split_axis=1, concat_axis=0, tiled=True)  119 us
    ppermute x2, waiting for transfers between devices, local(): lax.ppermute(branch, 'cb', [(dev, dev ^ hop) for dev in range(4)])  90.6 us
    all_gather x1, waiting for transfers between devices, local(): lax.all_gather(hidden, 'ra', axis=0, tiled=True)  66.4 us
    all_to_all x1, waiting for transfers between devices, local(): lax.all_to_all(w_gate, 'ra', split_axis=1, concat_axis=0, tiled=True)  22 us
    unnamed x12, local copies, waits for them, and re-layouts  16.7 us
  transfers between devices with their start and end apart: 6, of which 5 were waited for; matrix products, arithmetic and copies ran while one was open for 4% of the time, Pallas kernels for 0%

profile of v1, /device:TPU:0, one launch (start us, length us, event | category | flops | bytes accessed | tf_op | source)
XLA Modules:
  0.0 553.2 jit_solution(729006522425659918)
XLA Ops:
  6.5 8.3 %copy.11 = bf16[1024,2816]{0,1:T(8,128)(2,1)} copy(bf16[1024,2816]{1,0:T(8,128)(2,1)} %param.11) | data formatting | bytes 11534336 | tf_op args[3]
  14.8 6.3 %all-to-all-start.1 = ((bf16[1024,4,704]{0,2,1:T(8,128)(2,1)}), bf16[1024,4,704]{0,2,1:T(8,128)(2,1)}, u32[]{:S(2)}, u32[]{:S(2)}) async-start(bf16[1024,4,704]{0,2,1:T(8,128)(2,1)} %bitcast.26), calls=%async_computation.1 | async-start | bytes 11534336 | tf_op jit(solution)/shard_map/all_to_all | solution.py:31
  21.1 8.3 %copy.9 = bf16[1024,2816]{0,1:T(8,128)(2,1)} copy(bf16[1024,2816]{1,0:T(8,128)(2,1)} %param.10) | data formatting | bytes 11534336 | tf_op args[2]
  29.5 119.1 %all-to-all-done.1 = bf16[1024,4,704]{0,2,1:T(8,128)(2,1)} async-done(((bf16[1024,4,704]{0,2,1:T(8,128)(2,1)}), bf16[1024,4,704]{0,2,1:T(8,128)(2,1)}, u32[]{:S(2)}, u32[]{:S(2)}) %all-to-all-start.1) | async-done | bytes 5767200 | tf_op jit(solution)/shard_map/all_to_all | solution.py:31
  148.6 5.3 all-to-all-start
  154.0 1.3 fusion.3
  155.3 1.0 dynamic-slice_reduce_fusion.2
  156.3 163.7 %psum.14 = f32[512]{0:T(512)S(1)} all-reduce(f32[512]{0:T(512)S(1)} %get-tuple-element.17), channel_id=1, replica_groups=mesh['ra'=4,'cb'=4,'dp'=2] {'ra'}, use_global_device_ids=true, to_apply=%region_1.0 | all-reduce | flops 512 | bytes 4096 | tf_op jit(solution)/shard_map/psum | solution.py:26
  320.0 6.1 %copy.14 = bf16[4,88,8,1024]{3,2,0,1:T(8,128)(2,1)} copy(bf16[4,88,8,1024]{3,2,1,0:T(8,128)(2,1)} %bitcast.11) | data formatting | bytes 11534336 | tf_op jit(solution)/shard_map/all_to_all | solution.py:31
  326.1 22.0 %all-to-all-done = bf16[1024,4,704]{0,2,1:T(8,128)(2,1)} async-done(((bf16[1024,4,704]{0,2,1:T(8,128)(2,1)}), bf16[1024,4,704]{0,2,1:T(8,128)(2,1)}, u32[]{:S(2)}, u32[]{:S(2)}) %all-to-all-start) | async-done | bytes 5767200 | tf_op jit(solution)/shard_map/all_to_all | solution.py:30
  348.1 6.1 %copy.13 = bf16[4,88,8,1024]{3,2,0,1:T(8,128)(2,1)} copy(bf16[4,88,8,1024]{3,2,1,0:T(8,128)(2,1)} %bitcast.9) | data formatting | bytes 11534336 | tf_op jit(solution)/shard_map/all_to_all | solution.py:30
  354.3 6.6 %fusion.4 = f32[704,512]{1,0:T(8,128)S(1)} fusion(bf16[512,4096]{1,0:T(8,128)(2,1)} %all-gather.3.cloned.1.call-done, bf16[4096,704]{0,1:T(8,128)(2,1)} %bitcast.27, f32[512]{0:T(512)S(1)} %add_rsqrt_fusion.1), kind=kOutput, calls=%fused_computation.10 | convolution fusion | flops 2953150464 | bytes 11405312 | tf_op jit(solution)/shard_map/dot_general | solution.py:37
  361.0 3.2 fusion.5
  364.2 1.0 fusion.16
  365.2 2.8 fusion.14
  368.0 66.4 %all-gather.5.cloned.1.call-done = bf16[2816,512]{1,0:T(8,128)(2,1)} async-done(((bf16[704,512]{1,0:T(8,128)(2,1)}), bf16[2816,512]{1,0:T(8,128)(2,1)}) %all-gather.5.cloned.1.call-update) | async-done | bytes 2883600 | tf_op jit(solution)/shard_map/all_gather | solution.py:47
  434.5 6.1 %fusion.18 = f32[512,1024]{1,0:T(8,128)S(1)} fusion(bf16[2816,512]{1,0:T(8,128)(2,1)} %all-gather.5.cloned.1.call-done, bf16[2816,1024]{1,0:T(8,128)(2,1)} %param.14), kind=kOutput, calls=%fused_computation.33 | convolution fusion | flops 2952790016 | bytes 10747904 | tf_op jit(solution)/shard_map/dot_general | solution.py:46
  440.6 1.5 collective-permute-start
  442.1 45.7 %collective-permute-done = f32[512,1024]{1,0:T(8,128)S(1)} collective-permute-done((f32[512,1024]{1,0:T(8,128)S(1)}, f32[512,1024]{1,0:T(8,128)S(1)}, u32[]{:S(2)}, u32[]{:S(2)}) %collective-permute-start) | collective-permute-done | bytes 2097184 | tf_op jit(solution)/shard_map/ppermute | solution.py:54
  487.8 0.6 add.61
  488.4 1.5 collective-permute-start.1
  489.9 44.9 %collective-permute-done.1 = f32[512,1024]{1,0:T(8,128)S(1)} collective-permute-done((f32[512,1024]{1,0:T(8,128)S(1)}, f32[512,1024]{1,0:T(8,128)S(1)}, u32[]{:S(2)}, u32[]{:S(2)}) %collective-permute-start.1) | collective-permute-done | bytes 2097184 | tf_op jit(solution)/shard_map/ppermute | solution.py:54
  535.1 9.9 %psum.15 = f32[512]{0:T(512)S(1)} all-reduce(f32[512]{0:T(512)S(1)} %get-tuple-element.11), channel_id=1, replica_groups=mesh['ra'=4,'cb'=4,'dp'=2] {'ra'}, use_global_device_ids=true, to_apply=%region_3.0 | all-reduce | flops 512 | bytes 4096 | tf_op jit(solution)/shard_map/psum | solution.py:55
  545.0 1.4 fusion.15
  (18 shorter events, 0.6 us)
Async XLA Ops:
  14.8 133.8 %all-to-all-start.1 = ((bf16[1024,4,704]{0,2,1:T(8,128)(2,1)}), bf16[1024,4,704]{0,2,1:T(8,128)(2,1)}, u32[]{:S(2)}, u32[]{:S(2)}) async-start(bf16[1024,4,704]{0,2,1:T(8,128)(2,1)} %bitcast.26), calls=%async_computation.1 | async-start | bytes 11534336 | tf_op jit(solution)/shard_map/all_to_all | solution.py:31
  148.6 5.3 copy-start.1
  148.6 5.4 copy-start.2
  148.6 199.5 %all-to-all-start = ((bf16[1024,4,704]{0,2,1:T(8,128)(2,1)}), bf16[1024,4,704]{0,2,1:T(8,128)(2,1)}, u32[]{:S(2)}, u32[]{:S(2)}) async-start(bf16[1024,4,704]{0,2,1:T(8,128)(2,1)} %bitcast.25), calls=%async_computation | async-start | bytes 11534336 | tf_op jit(solution)/shard_map/all_to_all | solution.py:30
  153.9 200.4 %all-gather.3.cloned.1.call-start = ((), (), s32[]{:S(2)}) async-start(), calls=%async_computation.2 | async-start | bytes 5242880 | tf_op jit(solution)/shard_map/all_gather | solution.py:34
  155.3 279.2 %all-gather.5.cloned.1.call-start = ((), (), s32[]{:S(2)}) async-start(), calls=%async_computation.3 | async-start | bytes 3604480 | tf_op jit(solution)/shard_map/all_gather | solution.py:47
  354.3 6.6 %copy-start = (bf16[4,88,8,1024]{3,2,0,1:T(8,128)(2,1)S(1)}, bf16[4,88,8,1024]{3,2,0,1:T(8,128)(2,1)}, u32[]{:S(2)}) copy-start(bf16[4,88,8,1024]{3,2,0,1:T(8,128)(2,1)} %copy.13) | copy-start | bytes 17301508
  354.3 6.8 %copy-start.4 = (bf16[512,4096]{1,0:T(8,128)(2,1)S(1)}, bf16[512,4096]{1,0:T(8,128)(2,1)}, u32[]{:S(2)}) copy-start(bf16[512,4096]{1,0:T(8,128)(2,1)} %all-gather.3.cloned.1.call-done) | copy-start | bytes 12582916
  440.6 47.3 %collective-permute-start = (f32[512,1024]{1,0:T(8,128)S(1)}, f32[512,1024]{1,0:T(8,128)S(1)}, u32[]{:S(2)}, u32[]{:S(2)}) collective-permute-start(f32[512,1024]{1,0:T(8,128)S(1)} %fusion.18), channel_id=1, source_target_pairs={{0,2},{2,0},{4,6},{6,4},{1,3},{3,1},{5,7},{7,5},{8,10},{10,8},{12,... | collective-permute-start | bytes 6291464 | tf_op jit(solution)/shard_map/ppermute | solution.py:54
  488.4 56.6 %copy-start.3 = (f32[1024]{0:T(1024)S(1)}, f32[1024]{0:T(1024)}, u32[]{:S(2)}) copy-start(f32[1024]{0:T(1024)} %param.15) | copy-start | bytes 12292
  488.4 46.4 %collective-permute-start.1 = (f32[512,1024]{1,0:T(8,128)S(1)}, f32[512,1024]{1,0:T(8,128)S(1)}, u32[]{:S(2)}, u32[]{:S(2)}) collective-permute-start(f32[512,1024]{1,0:T(8,128)S(1)} %add.61), channel_id=1, source_target_pairs={{0,4},{2,6},{4,0},{6,2},{1,5},{3,7},{5,1},{7,3},{8,12},{10,14},{12... | collective-permute-start | bytes 6291464 | tf_op jit(solution)/shard_map/ppermute | solution.py:54
Sparse Core Ops, SparseCore 0:
  156.3 164.8 all-gather.2
  368.2 66.2 all-gather.4
